TPU v7x, 32 devices: a whole 2x2x4 slice. The times are simulated.
32 devices in a mesh: kv: 4 (over y, x), tp: 8 (over z, core).
Axes of the slice: x: 2, y: 2, z: 4, core: 2. Of those that a mesh axis runs over, the one named last changes fastest.
Arguments:
- tokens: bfloat16 [256, 4096], P(None, ('kv', 'tp')), may hold values from -10 to 10
- past_state: float32 [256, 32, 64, 128], P('kv', 'tp'), may hold values from -6 to 6
- first_gain: float32 [4096], P('kv'), may hold values from 0.1 to 1.9
- first_gate: bfloat16 [4096, 11264], P('kv', 'tp'), may hold values from -0.09375 to 0.09375
- first_up: bfloat16 [4096, 11264], P('kv', 'tp'), may hold values from -0.09375 to 0.09375
- first_down: bfloat16 [11264, 4096], P('tp', 'kv'), may hold values from -0.078125 to 0.078125
- mix_gain: float32 [4096], P('kv'), may hold values from 0.1 to 1.9
- query_weight: bfloat16 [4096, 2048], P('kv', 'tp'), may hold values from -0.09375 to 0.09375
- key_weight: bfloat16 [4096, 2048], P('kv', 'tp'), may hold values from -0.09375 to 0.09375
- value_weight: bfloat16 [4096, 4096], P('kv', 'tp'), may hold values from -0.09375 to 0.09375
- output_gate_weight: bfloat16 [4096, 4096], P('kv', 'tp'), may hold values from -0.09375 to 0.09375
- head_gain: float32 [4096], P('tp'), may hold values from 0.1 to 1.9
- out_weight: bfloat16 [4096, 4096], P('tp', 'kv'), may hold values from -0.125 to 0.125
- second_gain: float32 [4096], P('kv'), may hold values from 0.1 to 1.9
- second_gate: bfloat16 [4096, 11264], P('kv', 'tp'), may hold values from -0.09375 to 0.09375
- second_up: bfloat16 [4096, 11264], P('kv', 'tp'), may hold values from -0.09375 to 0.09375
- second_down: bfloat16 [11264, 4096], P('tp', 'kv'), may hold values from -0.078125 to 0.078125
Outputs:
- mixed: bfloat16 [256, 4096], P(None, ('kv', 'tp'))
- new_state: float32 [256, 32, 64, 128], P('kv', 'tp')
All inputs are finite; a program needn't handle non-finite values.
Results may differ from a plain program's by a relative error of at most 0.033.
Values may be sent and summed in bfloat16 or wider, within the bound.
A program may use at most 128 MiB of HBM per device.

v0:
```python
import jax
import jax.numpy as jnp
from jax import lax
from jax.sharding import PartitionSpec as P

D = 4096
HEADS = 32
HEAD_K = 64
HEAD_V = 128
POS = 16384
EPS_RMS = 1e-06
EPS_GROUP = 1e-05
ROPE_BASE = 10000.0


def rotate(vectors):
    half_width = vectors.shape[-1] // 2
    frequency = ROPE_BASE ** (-jnp.arange(half_width, dtype=jnp.float32) / half_width)
    angles = POS * frequency
    cosine = jnp.cos(angles)
    sine_part = jnp.sin(angles)
    lower = vectors[..., :half_width]
    upper = vectors[..., half_width:]
    return jnp.concatenate(
        [lower * cosine - upper * sine_part, lower * sine_part + upper * cosine], axis=-1
    )


def activate(gate_sum, up_sum, summed):
    inverse_rms = lax.rsqrt(summed / D + EPS_RMS)[:, None]
    return (jax.nn.silu(gate_sum * inverse_rms) * (up_sum * inverse_rms)).astype(jnp.bfloat16)


def channel_mix(widened, gain, w_gate, w_up, w_down):
    widened_f = widened.astype(jnp.float32)
    scaled = (widened_f * gain).astype(jnp.bfloat16)
    squares = jnp.sum(widened_f * widened_f, axis=1)
    gate_part = jnp.dot(scaled, w_gate, preferred_element_type=jnp.float32)
    up_part = jnp.dot(scaled, w_up, preferred_element_type=jnp.float32)
    gate_sum, up_sum, summed = (
        lax.psum(gate_part.astype(jnp.bfloat16), "kv").astype(jnp.float32),
        lax.psum(up_part.astype(jnp.bfloat16), "kv").astype(jnp.float32),
        lax.psum(squares.astype(jnp.bfloat16), "kv").astype(jnp.float32),
    )
    return 0.5 * jnp.dot(
        activate(gate_sum, up_sum, summed), w_down, preferred_element_type=jnp.float32
    )


def token_mix(
    widened,
    past_state,
    gain,
    query_weight,
    key_weight,
    value_weight,
    output_gate_weight,
    head_gain,
    out_weight,
):
    widened_f = widened.astype(jnp.float32)
    scaled = (widened_f * gain).astype(jnp.bfloat16)
    squares = jnp.sum(widened_f * widened_f, axis=1)
    query_part = jnp.dot(scaled, query_weight, preferred_element_type=jnp.float32)
    key_part = jnp.dot(scaled, key_weight, preferred_element_type=jnp.float32)
    value_part = jnp.dot(scaled, value_weight, preferred_element_type=jnp.float32)
    gate_part = jnp.dot(scaled, output_gate_weight, preferred_element_type=jnp.float32)
    queries, keys_now, values_now, gate_now, summed = (
        lax.psum_scatter(
            query_part.astype(jnp.bfloat16), "kv", scatter_dimension=0, tiled=True
        ).astype(jnp.float32),
        lax.psum_scatter(
            key_part.astype(jnp.bfloat16), "kv", scatter_dimension=0, tiled=True
        ).astype(jnp.float32),
        lax.psum_scatter(
            value_part.astype(jnp.bfloat16), "kv", scatter_dimension=0, tiled=True
        ).astype(jnp.float32),
        lax.psum_scatter(
            gate_part.astype(jnp.bfloat16), "kv", scatter_dimension=0, tiled=True
        ).astype(jnp.float32),
        lax.psum_scatter(
            squares.astype(jnp.bfloat16), "kv", scatter_dimension=0, tiled=True
        ).astype(jnp.float32),
    )
    inverse_rms = lax.rsqrt(summed / D + EPS_RMS)[:, None]
    row_count = past_state.shape[0]
    local_heads = past_state.shape[1]
    queries = rotate((queries * inverse_rms).reshape(row_count, local_heads, HEAD_K)) * HEAD_K ** (
        -0.5
    )
    keys_now = rotate((keys_now * inverse_rms).reshape(row_count, local_heads, HEAD_K))
    values_now = (values_now * inverse_rms).reshape(row_count, local_heads, HEAD_V)
    gate_now = gate_now * inverse_rms
    head_level = (lax.axis_index("tp") * local_heads + jnp.arange(local_heads)).astype(jnp.float32)
    retained = 1.0 - jnp.exp2(-5.0 - 16.0 * head_level / (HEADS - 1))
    new_state = (
        retained[None, :, None, None] * past_state
        + keys_now[:, :, :, None] * values_now[:, :, None, :]
    )
    retrieved = jnp.einsum("bhk,bhkv->bhv", queries, new_state, precision=lax.Precision.HIGHEST)
    head_mean = jnp.mean(retrieved, axis=-1, keepdims=True)
    variance = jnp.mean(jnp.square(retrieved - head_mean), axis=-1, keepdims=True)
    normed = ((retrieved - head_mean) * lax.rsqrt(variance + EPS_GROUP)).reshape(
        row_count, local_heads * HEAD_V
    )
    mixed_heads = (jax.nn.silu(gate_now) * (normed * head_gain)).astype(jnp.bfloat16)
    projected = jnp.dot(
        lax.all_gather(mixed_heads, "kv", axis=0, tiled=True),
        out_weight,
        preferred_element_type=jnp.float32,
    )
    return (projected, new_state)


def shards(
    tokens,
    past_state,
    first_gain,
    first_gate,
    first_up,
    first_down,
    mix_gain,
    query_weight,
    key_weight,
    value_weight,
    output_gate_weight,
    head_gain,
    out_weight,
    second_gain,
    second_gate,
    second_up,
    second_down,
):

    def first_section(widened):
        return (channel_mix(widened, first_gain, first_gate, first_up, first_down), None)

    def middle_section(widened):
        return token_mix(
            widened,
            past_state,
            mix_gain,
            query_weight,
            key_weight,
            value_weight,
            output_gate_weight,
            head_gain,
            out_weight,
        )

    def last_section(widened):
        return (channel_mix(widened, second_gain, second_gate, second_up, second_down), None)

    sections = [first_section, middle_section, last_section]
    own_columns = tokens
    widened = lax.all_gather(tokens, "tp", axis=1, tiled=True)
    state_out = past_state
    for section_index in range(3):
        branch_out, produced = sections[section_index](widened)
        if produced is not None:
            state_out = produced
        own_piece = lax.psum_scatter(
            branch_out.astype(jnp.bfloat16), "tp", scatter_dimension=1, tiled=True
        ).astype(jnp.float32)
        own_columns = (own_columns.astype(jnp.float32) + own_piece).astype(jnp.bfloat16)
        if section_index < 2:
            widened = lax.all_gather(own_columns, "tp", axis=1, tiled=True)
    return (own_columns, state_out)


def solution(mesh):
    in_specs = (
        P(None, ("kv", "tp")),
        P("kv", "tp", None, None),
        P("kv"),
        P("kv", "tp"),
        P("kv", "tp"),
        P("tp", "kv"),
        P("kv"),
        P("kv", "tp"),
        P("kv", "tp"),
        P("kv", "tp"),
        P("kv", "tp"),
        P("tp"),
        P("tp", "kv"),
        P("kv"),
        P("kv", "tp"),
        P("kv", "tp"),
        P("tp", "kv"),
    )
    out_specs = (P(None, ("kv", "tp")), P("kv", "tp", None, None))
    return jax.shard_map(shards, mesh=mesh, in_specs=in_specs, out_specs=out_specs, check_vma=False)
```

profile of v0, /device:TPU:0, one launch (start us, length us, event | category | flops | bytes accessed | tf_op | source)
XLA Modules:
  0.0 409.7 jit_solution(10858656113238108868)
XLA Ops:
  7.2 15.8 %all_gather.12 = bf16[256,1024]{1,0:T(8,128)(2,1)S(1)} all-gather(bf16[256,128]{1,0:T(8,128)(2,1)} %param.17), channel_id=1, replica_groups=mesh['kv'=4,'tp'=8] {'tp'}, dimensions={1}, use_global_device_ids=true | all-gather | bytes 589824 | tf_op jit(solution)/shard_map/all_gather | solution.py:156
  23.0 2.5 convolution_convert_fusion.2
  25.6 1.9 convolution_convert_fusion.3
  27.7 10.1 %psum.43 = bf16[256]{0:T(256)(128)(2,1)S(1)} all-reduce(bf16[256]{0:T(256)(128)(2,1)S(1)} %fusion.3), channel_id=1, replica_groups=mesh['kv'=4,'tp'=8] {'kv'}, use_global_device_ids=true, to_apply=%region_2.0 | all-reduce | flops 256 | bytes 1024 | tf_op jit(solution)/shard_map/psum | solution.py:43
  37.8 48.4 %all-reduce.8.cloned.1.call-done = (bf16[256,1408]{1,0:T(8,128)(2,1)}, bf16[256,1408]{1,0:T(8,128)(2,1)}) async-done(((bf16[256,1408]{1,0:T(8,128)(2,1)}, bf16[256,1408]{1,0:T(8,128)(2,1)}), (bf16[256,1408]{1,0:T(8,128)(2,1)}, bf16[256,1408]{1,0:T(8,128)(2,1)})) %all-reduce.8.cloned.1.call-update) | async-done | bytes 1441808 | tf_op jit(solution)/shard_map/psum | solution.py:42
  86.2 3.5 fusion
  89.7 1.0 copy.24
  90.8 31.2 %reduce-scatter.22.cloned.1.call-done = bf16[128,256]{1,0:T(8,128)(2,1)} async-done(((bf16[1024,256]{1,0:T(8,128)(2,1)}), bf16[128,256]{1,0:T(8,128)(2,1)}) %reduce-scatter.22.cloned.1.call-update) | async-done | bytes 65552
  123.0 14.0 %all_gather.13 = bf16[256,1024]{1,0:T(8,128)(2,1)S(1)} all-gather(bf16[256,128]{1,0:T(8,128)(2,1)S(1)} %add_convert_fusion.2), channel_id=1, replica_groups=mesh['kv'=4,'tp'=8] {'tp'}, dimensions={1}, use_global_device_ids=true | all-gather | bytes 589824 | tf_op jit(solution)/shard_map/all_gather | solution.py:167
  137.1 2.0 convolution_convert_fusion.8
  140.4 2.0 convolution_convert_fusion.7
  142.5 2.4 convolution_convert_fusion.5
  145.1 9.9 %all-reduce = bf16[256]{0:T(256)(128)(2,1)S(1)} all-reduce(bf16[256]{0:T(256)(128)(2,1)S(1)} %fusion.5), channel_id=4, replica_groups=mesh['kv'=4,'tp'=8] {'kv'}, use_global_device_ids=true, to_apply=%region_7.8.clone | all-reduce | flops 256 | bytes 1024
  155.2 2.4 convolution_convert_fusion.6
  157.8 4.2 %reduce-scatter.16.cloned.1.call-done = bf16[64,256]{1,0:T(8,128)(2,1)} async-done(((bf16[256,256]{1,0:T(8,128)(2,1)}), bf16[64,256]{1,0:T(8,128)(2,1)}) %reduce-scatter.16.cloned.1.call-update) | async-done | bytes 32784 | tf_op jit(solution)/shard_map/reduce_scatter | solution.py:69
  162.0 26.8 %reduce-scatter.18.cloned.1.call-done = bf16[64,256]{1,0:T(8,128)(2,1)} async-done(((bf16[256,256]{1,0:T(8,128)(2,1)}), bf16[64,256]{1,0:T(8,128)(2,1)}) %reduce-scatter.18.cloned.1.call-update) | async-done | bytes 32784 | tf_op jit(solution)/shard_map/reduce_scatter | solution.py:72
  190.2 26.1 %reduce-scatter.20.cloned.1.call-done = bf16[64,512]{1,0:T(8,128)(2,1)} async-done(((bf16[256,512]{1,0:T(8,128)(2,1)}), bf16[64,512]{1,0:T(8,128)(2,1)}) %reduce-scatter.20.cloned.1.call-update) | async-done | bytes 65552 | tf_op jit(solution)/shard_map/reduce_scatter | solution.py:75
  217.3 5.3 %multiply_add_fusion = f32[64,4,64,128]{3,2,1,0:T(8,128)S(1)} fusion(f32[64,4,64,128]{3,2,1,0:T(8,128)} %param.18, f32[64,4,128]{2,1,0:T(4,128)S(1)} %mul.290, f32[64,4,64]{2,1,0:T(4,128)S(1)} %copy.21, f32[4]{0:T(128)S(1)} %exponential_subtract_fusion), kind=kLoop, calls=%fused_computation | loop fusion | flops 6291456 | bytes 16973840 | tf_op jit(solution)/shard_map/add | solution.py:97
  222.6 7.3 %fusion.30 = f32[64,4,1,128]{3,2,1,0:T(1,128)S(1)} fusion(f32[64,4,64,1]{2,3,1,0:T(1,128)S(1)} %copy.22, f32[64,4,64,128]{3,2,1,0:T(8,128)S(1)} %multiply_add_fusion), kind=kOutput, calls=%fused_computation.64 | convolution fusion | flops 25165824 | bytes 8585216 | tf_op jit(solution)/shard_map/bhk,bhkv->bhv/dot_general | solution.py:100
  230.6 12.7 %reduce-scatter.14.cloned.1.call-done = bf16[64,512]{1,0:T(8,128)(2,1)} async-done(((bf16[256,512]{1,0:T(8,128)(2,1)}), bf16[64,512]{1,0:T(8,128)(2,1)}) %reduce-scatter.14.cloned.1.call-update) | async-done | bytes 65552 | tf_op jit(solution)/shard_map/reduce_scatter | solution.py:78
  244.3 9.3 %all_gather.14 = bf16[256,512]{1,0:T(8,128)(2,1)S(1)} all-gather(bf16[64,512]{1,0:T(8,128)(2,1)S(1)} %fusion.21), channel_id=1, replica_groups=mesh['kv'=4,'tp'=8] {'kv'}, dimensions={0}, use_global_device_ids=true | all-gather | bytes 327680 | tf_op jit(solution)/shard_map/all_gather | solution.py:108
  253.6 1.7 convolution_convert_fusion.4
  255.2 1.0 copy.26
  256.3 31.4 %reduce-scatter.24.cloned.1.call-done = bf16[128,256]{1,0:T(8,128)(2,1)} async-done(((bf16[1024,256]{1,0:T(8,128)(2,1)}), bf16[128,256]{1,0:T(8,128)(2,1)}) %reduce-scatter.24.cloned.1.call-update) | async-done | bytes 65552
  288.7 14.2 %all_gather.15 = bf16[256,1024]{1,0:T(8,128)(2,1)S(1)} all-gather(bf16[256,128]{1,0:T(8,128)(2,1)S(1)} %add_convert_fusion.1), channel_id=1, replica_groups=mesh['kv'=4,'tp'=8] {'tp'}, dimensions={1}, use_global_device_ids=true | all-gather | bytes 589824 | tf_op jit(solution)/shard_map/all_gather | solution.py:167
  302.8 3.7 convolution_convert_fusion
  306.5 1.9 convolution_convert_fusion.1
  308.6 10.2 %psum.46 = bf16[256]{0:T(256)(128)(2,1)S(1)} all-reduce(bf16[256]{0:T(256)(128)(2,1)S(1)} %fusion.7), channel_id=1, replica_groups=mesh['kv'=4,'tp'=8] {'kv'}, use_global_device_ids=true, to_apply=%region_16.17 | all-reduce | flops 256 | bytes 1024 | tf_op jit(solution)/shard_map/psum | solution.py:43
  318.9 46.7 %all-reduce.6.cloned.1.call-done = (bf16[256,1408]{1,0:T(8,128)(2,1)}, bf16[256,1408]{1,0:T(8,128)(2,1)}) async-done(((bf16[256,1408]{1,0:T(8,128)(2,1)}, bf16[256,1408]{1,0:T(8,128)(2,1)}), (bf16[256,1408]{1,0:T(8,128)(2,1)}, bf16[256,1408]{1,0:T(8,128)(2,1)})) %all-reduce.6.cloned.1.call-update) | async-done | bytes 1441808 | tf_op jit(solution)/shard_map/psum | solution.py:42
  365.6 3.4 fusion.1
  369.0 1.0 copy.28
  370.0 31.6 %reduce-scatter.26.cloned.1.call-done = bf16[128,256]{1,0:T(8,128)(2,1)} async-done(((bf16[1024,256]{1,0:T(8,128)(2,1)}), bf16[128,256]{1,0:T(8,128)(2,1)}) %reduce-scatter.26.cloned.1.call-update) | async-done | bytes 65552
  (69 shorter events, 9.5 us)
Async XLA Ops:
  7.2 15.9 %copy-start = (bf16[1024,1408]{1,0:T(8,128)(2,1)S(1)}, bf16[1024,1408]{1,0:T(8,128)(2,1)}, u32[]{:S(2)}) copy-start(bf16[1024,1408]{1,0:T(8,128)(2,1)} %param.21) | copy-start | bytes 8650756
  7.2 18.4 %copy-start.6 = (f32[1024]{0:T(1024)S(1)}, f32[1024]{0:T(1024)}, u32[]{:S(2)}) copy-start(f32[1024]{0:T(1024)} %param.19) | copy-start | bytes 12292
  7.2 79.0 %all-reduce.8.cloned.1.call-start = ((), (), s32[]{:S(2)}) async-start(), calls=%async_computation.15 | async-start | bytes 2883584 | tf_op jit(solution)/shard_map/psum | solution.py:42
  7.2 18.3 %copy-start.4 = (bf16[1024,1408]{1,0:T(8,128)(2,1)S(1)}, bf16[1024,1408]{1,0:T(8,128)(2,1)}, u32[]{:S(2)}) copy-start(bf16[1024,1408]{1,0:T(8,128)(2,1)} %param.20) | copy-start | bytes 8650756
  27.5 94.6 %reduce-scatter.22.cloned.1.call-start = ((), (), s32[]{:S(2)}) async-start(), calls=%async_computation.11 | async-start | bytes 589824
  86.2 36.8 %copy-start.2 = (bf16[256,128]{1,0:T(8,128)(2,1)S(1)}, bf16[256,128]{1,0:T(8,128)(2,1)}, u32[]{:S(2)}) copy-start(bf16[256,128]{1,0:T(8,128)(2,1)} %param.17) | copy-start | bytes 196612
  86.2 50.9 %copy-start.7 = (f32[1024]{0:T(1024)S(1)}, f32[1024]{0:T(1024)}, u32[]{:S(2)}) copy-start(f32[1024]{0:T(1024)} %param.23) | copy-start | bytes 12292
  89.7 49.5 %copy-start.9 = (u32[32]{0:T(128)S(1)}, u32[32]{0:T(128)}, u32[]{:S(2)}) copy-start(u32[32]{0:T(128)} %constant.53) | copy-start | bytes 388
  90.7 71.3 %reduce-scatter.16.cloned.1.call-start = ((), (), s32[]{:S(2)}) async-start(), calls=%async_computation.8 | async-start | bytes 163840 | tf_op jit(solution)/shard_map/reduce_scatter | solution.py:69
  139.1 49.7 %reduce-scatter.18.cloned.1.call-start = ((), (), s32[]{:S(2)}) async-start(), calls=%async_computation.9 | async-start | bytes 163840 | tf_op jit(solution)/shard_map/reduce_scatter | solution.py:72
  142.4 73.9 %reduce-scatter.20.cloned.1.call-start = ((), (), s32[]{:S(2)}) async-start(), calls=%async_computation.10 | async-start | bytes 327680 | tf_op jit(solution)/shard_map/reduce_scatter | solution.py:75
  144.9 98.4 %reduce-scatter.14.cloned.1.call-start = ((), (), s32[]{:S(2)}) async-start(), calls=%async_computation.7 | async-start | bytes 327680 | tf_op jit(solution)/shard_map/reduce_scatter | solution.py:78
  157.6 130.1 %reduce-scatter.24.cloned.1.call-start = ((), (), s32[]{:S(2)}) async-start(), calls=%async_computation.12 | async-start | bytes 589824
  222.6 7.4 %copy-start.1 = (f32[64,4,64,128]{3,2,1,0:T(8,128)}, f32[64,4,64,128]{3,2,1,0:T(8,128)S(1)}, u32[]{:S(2)}) copy-start(f32[64,4,64,128]{3,2,1,0:T(8,128)S(1)} %multiply_add_fusion) | copy-start | bytes 25165828
  222.6 20.7 %copy-start.3 = (f32[512]{0:T(512)S(1)}, f32[512]{0:T(512)}, u32[]{:S(2)}) copy-start(f32[512]{0:T(512)} %param.28) | copy-start | bytes 6148
  230.0 72.8 %copy-start.8 = (f32[1024]{0:T(1024)S(1)}, f32[1024]{0:T(1024)}, u32[]{:S(2)}) copy-start(f32[1024]{0:T(1024)} %param.30) | copy-start | bytes 12292
  256.2 109.3 %all-reduce.6.cloned.1.call-start = ((), (), s32[]{:S(2)}) async-start(), calls=%async_computation.14 | async-start | bytes 2883584 | tf_op jit(solution)/shard_map/psum | solution.py:42
  288.6 17.9 %copy-start.5 = (bf16[1024,1408]{1,0:T(8,128)(2,1)S(1)}, bf16[1024,1408]{1,0:T(8,128)(2,1)}, u32[]{:S(2)}) copy-start(bf16[1024,1408]{1,0:T(8,128)(2,1)} %param.31) | copy-start | bytes 8650756
  308.4 93.2 %reduce-scatter.26.cloned.1.call-start = ((), (), s32[]{:S(2)}) async-start(), calls=%async_computation.13 | async-start | bytes 589824
Sparse Core Ops, SparseCore 0:
  27.6 58.5 all-reduce.7
  90.8 31.1 reduce-scatter.21
  139.2 22.7 reduce-scatter.15
  164.6 24.1 reduce-scatter.17
  192.0 24.3 reduce-scatter.19
  218.9 24.3 reduce-scatter.13
  256.4 31.2 reduce-scatter.23
  308.5 56.9 all-reduce.5
  370.1 31.3 reduce-scatter.25
where the time goes:
time: 411 us; the launch traced here: 410 us
  waiting for transfers between devices  259 us (63%)
  blocking collectives  83.5 us (20%)
  matrix products  34.6 us (8%)
  between operations  14.8 us (4%)
  other arithmetic  10.2 us (2%)
  local copies, waits for them, and re-layouts  6.92 us (2%)
    psum x2, waiting for transfers between devices, channel_mix(): lax.psum(up_part.astype(jnp.bfloat16), 'kv').astype(jnp.float32)  95.1 us
    unnamed x12, waiting for transfers between devices  94.3 us
    all_gather x2, blocking collectives, shards(): widened = lax.all_gather(own_columns, 'tp', axis=1, tiled=True)  28.2 us
    reduce_scatter x1, waiting for transfers between devices, token_mix(): lax.psum_scatter(key_part.astype(jnp.bfloat16), 'kv', scatter_dimension=0...  26.8 us
    reduce_scatter x1, waiting for transfers between devices, token_mix(): lax.psum_scatter(value_part.astype(jnp.bfloat16), 'kv', scatter_dimension...  26.1 us
    psum x2, blocking collectives, channel_mix(): lax.psum(squares.astype(jnp.bfloat16), 'kv').astype(jnp.float32)  20.3 us
    all_gather x1, blocking collectives, shards(): widened = lax.all_gather(tokens, 'tp', axis=1, tiled=True)  15.8 us
    reduce_scatter x1, waiting for transfers between devices, token_mix(): lax.psum_scatter(gate_part.astype(jnp.bfloat16), 'kv', scatter_dimension=...  12.7 us
  transfers between devices with their start and end apart: 9, of which 9 were waited for; matrix products, arithmetic and copies ran while one was open for 6% of the time, Pallas kernels for 0%

commit v1 on v0

--- a/solution.py
+++ b/solution.py
@@ -39,7 +39,7 @@
     up_part = jnp.dot(scaled, w_up, preferred_element_type=jnp.float32)
     gate_sum, up_sum, summed = (
         lax.psum(gate_part.astype(jnp.bfloat16), "kv").astype(jnp.float32),
-        lax.psum(up_part.astype(jnp.bfloat16), "kv").astype(jnp.float32),
+        jnp.sum(lax.all_gather(up_part.astype(jnp.bfloat16), "kv"), axis=0).astype(jnp.float32),
         lax.psum(squares.astype(jnp.bfloat16), "kv").astype(jnp.float32),
     )
     return 0.5 * jnp.dot(

time: 411 us -> 474 us (1.15)
  waiting for transfers between devices: 259 us -> 313 us
  other arithmetic: 10.2 us -> 16.7 us
    all_gather x0 -> x2, waiting for transfers between devices: none -> 53.5 us  [channel_mix(): lax.all_gather(up_part.astype(jnp.bfloat16), 'kv')]
    reduce_sum x0 -> x2, other arithmetic: none -> 6.58 us  [channel_mix(): jnp.sum(lax.all_gather(up_part.astype(jnp.bfloat16), 'kv'), axis=0)]
    unnamed x12 -> x14, waiting for transfers between devices: 94.3 us -> 94.6 us
  transfers between devices with their start and end apart: 9 -> 11, of which waited for: 9 -> 11; matrix products, arithmetic and copies ran while one was open for 6% -> 8% of each run, Pallas kernels for 0% -> 0%
where the time goes in v1:
time: 474 us; the launch traced here: 473 us
  waiting for transfers between devices  313 us (66%)
  blocking collectives  83.4 us (18%)
  matrix products  38.2 us (8%)
  other arithmetic  16.7 us (4%)
  between operations  14.8 us (3%)
  local copies, waits for them, and re-layouts  6.91 us (1%)
    psum x2, waiting for transfers between devices, channel_mix(): lax.psum(gate_part.astype(jnp.bfloat16), 'kv').astype(jnp.float32)  94.8 us
    unnamed x14, waiting for transfers between devices  94.6 us
    all_gather x2, waiting for transfers between devices, channel_mix(): lax.all_gather(up_part.astype(jnp.bfloat16), 'kv')  53.5 us
    all_gather x2, blocking collectives, shards(): widened = lax.all_gather(own_columns, 'tp', axis=1, tiled=True)  28 us
    reduce_scatter x1, waiting for transfers between devices, token_mix(): lax.psum_scatter(key_part.astype(jnp.bfloat16), 'kv', scatter_dimension=0...  26.8 us
    reduce_scatter x1, waiting for transfers between devices, token_mix(): lax.psum_scatter(value_part.astype(jnp.bfloat16), 'kv', scatter_dimension...  26.1 us
    psum x2, blocking collectives, channel_mix(): lax.psum(squares.astype(jnp.bfloat16), 'kv').astype(jnp.float32)  20.6 us
    all_gather x1, blocking collectives, shards(): widened = lax.all_gather(tokens, 'tp', axis=1, tiled=True)  15.8 us
  transfers between devices with their start and end apart: 11, of which 11 were waited for; matrix products, arithmetic and copies ran while one was open for 8% of the time, Pallas kernels for 0%

profile of v1, /device:TPU:0, one launch (start us, length us, event | category | flops | bytes accessed | tf_op | source)
XLA Modules:
  0.0 473.5 jit_solution(7350168983002603778)
XLA Ops:
  7.2 15.8 %all_gather.24 = bf16[256,1024]{1,0:T(8,128)(2,1)S(1)} all-gather(bf16[256,128]{1,0:T(8,128)(2,1)} %param.17), channel_id=1, replica_groups=mesh['kv'=4,'tp'=8] {'tp'}, dimensions={1}, use_global_device_ids=true | all-gather | bytes 589824 | tf_op jit(solution)/shard_map/all_gather | solution.py:156
  23.0 2.6 convolution_convert_fusion.2
  25.7 3.7 convolution_convert_fusion.3
  29.6 10.2 %psum.29 = bf16[256]{0:T(256)(128)(2,1)S(1)} all-reduce(bf16[256]{0:T(256)(128)(2,1)S(1)} %fusion.3), channel_id=1, replica_groups=mesh['kv'=4,'tp'=8] {'kv'}, use_global_device_ids=true, to_apply=%region_2.0 | all-reduce | flops 256 | bytes 1024 | tf_op jit(solution)/shard_map/psum | solution.py:43
  39.9 27.5 %all-gather.5.cloned.1.call-done = bf16[1024,1408]{1,0:T(8,128)(2,1)} async-done(((bf16[256,1408]{1,0:T(8,128)(2,1)}), bf16[1024,1408]{1,0:T(8,128)(2,1)}) %all-gather.5.cloned.1.call-update) | async-done | bytes 2883600 | tf_op jit(solution)/shard_map/all_gather | solution.py:42
  67.4 3.3 reduce_sum.70
  70.7 47.5 %all-reduce.4.cloned.1.call-done = bf16[256,1408]{1,0:T(8,128)(2,1)} async-done(((bf16[256,1408]{1,0:T(8,128)(2,1)}), bf16[256,1408]{1,0:T(8,128)(2,1)}) %all-reduce.4.cloned.1.call-update) | async-done | bytes 720912 | tf_op jit(solution)/shard_map/psum | solution.py:41
  118.2 3.4 fusion
  122.8 31.5 %reduce-scatter.22.cloned.1.call-done = bf16[128,256]{1,0:T(8,128)(2,1)} async-done(((bf16[1024,256]{1,0:T(8,128)(2,1)}), bf16[128,256]{1,0:T(8,128)(2,1)}) %reduce-scatter.22.cloned.1.call-update) | async-done | bytes 65552
  155.2 14.0 %all_gather.27 = bf16[256,1024]{1,0:T(8,128)(2,1)S(1)} all-gather(bf16[256,128]{1,0:T(8,128)(2,1)S(1)} %add_convert_fusion.2), channel_id=1, replica_groups=mesh['kv'=4,'tp'=8] {'tp'}, dimensions={1}, use_global_device_ids=true | all-gather | bytes 589824 | tf_op jit(solution)/shard_map/all_gather | solution.py:167
  169.2 2.0 convolution_convert_fusion.8
  172.6 2.0 convolution_convert_fusion.7
  174.7 2.4 convolution_convert_fusion.5
  177.3 9.7 %all-reduce = bf16[256]{0:T(256)(128)(2,1)S(1)} all-reduce(bf16[256]{0:T(256)(128)(2,1)S(1)} %fusion.5), channel_id=6, replica_groups=mesh['kv'=4,'tp'=8] {'kv'}, use_global_device_ids=true, to_apply=%region_7.8.clone | all-reduce | flops 256 | bytes 1024
  187.1 2.4 convolution_convert_fusion.6
  189.7 4.2 reduce-scatter.16.cloned.1.call-done
  193.9 26.8 %reduce-scatter.18.cloned.1.call-done = bf16[64,256]{1,0:T(8,128)(2,1)} async-done(((bf16[256,256]{1,0:T(8,128)(2,1)}), bf16[64,256]{1,0:T(8,128)(2,1)}) %reduce-scatter.18.cloned.1.call-update) | async-done | bytes 32784 | tf_op jit(solution)/shard_map/reduce_scatter | solution.py:72
  222.1 26.1 %reduce-scatter.20.cloned.1.call-done = bf16[64,512]{1,0:T(8,128)(2,1)} async-done(((bf16[256,512]{1,0:T(8,128)(2,1)}), bf16[64,512]{1,0:T(8,128)(2,1)}) %reduce-scatter.20.cloned.1.call-update) | async-done | bytes 65552 | tf_op jit(solution)/shard_map/reduce_scatter | solution.py:75
  249.2 5.3 %multiply_add_fusion = f32[64,4,64,128]{3,2,1,0:T(8,128)S(1)} fusion(f32[64,4,64,128]{3,2,1,0:T(8,128)} %param.18, f32[64,4,128]{2,1,0:T(4,128)S(1)} %mul.290, f32[64,4,64]{2,1,0:T(4,128)S(1)} %copy.21, f32[4]{0:T(128)S(1)} %exponential_subtract_fusion), kind=kLoop, calls=%fused_computation | loop fusion | flops 6291456 | bytes 16973840 | tf_op jit(solution)/shard_map/add | solution.py:97
  254.5 7.3 %fusion.30 = f32[64,4,1,128]{3,2,1,0:T(1,128)S(1)} fusion(f32[64,4,64,1]{2,3,1,0:T(1,128)S(1)} %copy.22, f32[64,4,64,128]{3,2,1,0:T(8,128)S(1)} %multiply_add_fusion), kind=kOutput, calls=%fused_computation.64 | convolution fusion | flops 25165824 | bytes 8585216 | tf_op jit(solution)/shard_map/bhk,bhkv->bhv/dot_general | solution.py:100
  262.5 12.8 %reduce-scatter.14.cloned.1.call-done = bf16[64,512]{1,0:T(8,128)(2,1)} async-done(((bf16[256,512]{1,0:T(8,128)(2,1)}), bf16[64,512]{1,0:T(8,128)(2,1)}) %reduce-scatter.14.cloned.1.call-update) | async-done | bytes 65552 | tf_op jit(solution)/shard_map/reduce_scatter | solution.py:78
  276.3 9.3 %all_gather.28 = bf16[256,512]{1,0:T(8,128)(2,1)S(1)} all-gather(bf16[64,512]{1,0:T(8,128)(2,1)S(1)} %fusion.21), channel_id=1, replica_groups=mesh['kv'=4,'tp'=8] {'kv'}, dimensions={0}, use_global_device_ids=true | all-gather | bytes 327680 | tf_op jit(solution)/shard_map/all_gather | solution.py:108
  288.3 31.4 %reduce-scatter.24.cloned.1.call-done = bf16[128,256]{1,0:T(8,128)(2,1)} async-done(((bf16[1024,256]{1,0:T(8,128)(2,1)}), bf16[128,256]{1,0:T(8,128)(2,1)}) %reduce-scatter.24.cloned.1.call-update) | async-done | bytes 65552
  320.7 14.0 %all_gather.29 = bf16[256,1024]{1,0:T(8,128)(2,1)S(1)} all-gather(bf16[256,128]{1,0:T(8,128)(2,1)S(1)} %add_convert_fusion.1), channel_id=1, replica_groups=mesh['kv'=4,'tp'=8] {'tp'}, dimensions={1}, use_global_device_ids=true | all-gather | bytes 589824 | tf_op jit(solution)/shard_map/all_gather | solution.py:167
  334.8 3.7 convolution_convert_fusion
  338.5 3.7 convolution_convert_fusion.1
  342.4 10.3 %psum.31 = bf16[256]{0:T(256)(128)(2,1)S(1)} all-reduce(bf16[256]{0:T(256)(128)(2,1)S(1)} %fusion.7), channel_id=1, replica_groups=mesh['kv'=4,'tp'=8] {'kv'}, use_global_device_ids=true, to_apply=%region_16.17 | all-reduce | flops 256 | bytes 1024 | tf_op jit(solution)/shard_map/psum | solution.py:43
  352.8 25.9 %all-gather.7.cloned.1.call-done = bf16[1024,1408]{1,0:T(8,128)(2,1)} async-done(((bf16[256,1408]{1,0:T(8,128)(2,1)}), bf16[1024,1408]{1,0:T(8,128)(2,1)}) %all-gather.7.cloned.1.call-update) | async-done | bytes 2883600 | tf_op jit(solution)/shard_map/all_gather | solution.py:42
  378.7 3.3 reduce_sum.75
  382.0 47.3 %all-reduce.6.cloned.1.call-done = bf16[256,1408]{1,0:T(8,128)(2,1)} async-done(((bf16[256,1408]{1,0:T(8,128)(2,1)}), bf16[256,1408]{1,0:T(8,128)(2,1)}) %all-reduce.6.cloned.1.call-update) | async-done | bytes 720912 | tf_op jit(solution)/shard_map/psum | solution.py:41
  429.3 3.4 fusion.1
  433.8 31.6 %reduce-scatter.26.cloned.1.call-done = bf16[128,256]{1,0:T(8,128)(2,1)} async-done(((bf16[1024,256]{1,0:T(8,128)(2,1)}), bf16[128,256]{1,0:T(8,128)(2,1)}) %reduce-scatter.26.cloned.1.call-update) | async-done | bytes 65552
  (73 shorter events, 14.2 us)
Async XLA Ops:
  7.2 15.9 %copy-start = (bf16[1024,1408]{1,0:T(8,128)(2,1)S(1)}, bf16[1024,1408]{1,0:T(8,128)(2,1)}, u32[]{:S(2)}) copy-start(bf16[1024,1408]{1,0:T(8,128)(2,1)} %param.21) | copy-start | bytes 8650756
  7.2 60.2 %all-gather.5.cloned.1.call-start = ((), (), s32[]{:S(2)}) async-start(), calls=%async_computation.13 | async-start | bytes 3604480 | tf_op jit(solution)/shard_map/all_gather | solution.py:42
  23.0 2.7 copy-start.4
  25.6 92.5 %all-reduce.4.cloned.1.call-start = ((), (), s32[]{:S(2)}) async-start(), calls=%async_computation.7 | async-start | bytes 1441792 | tf_op jit(solution)/shard_map/psum | solution.py:41
  29.4 124.8 %reduce-scatter.22.cloned.1.call-start = ((), (), s32[]{:S(2)}) async-start(), calls=%async_computation.15 | async-start | bytes 589824
  70.7 84.5 %copy-start.2 = (bf16[256,128]{1,0:T(8,128)(2,1)S(1)}, bf16[256,128]{1,0:T(8,128)(2,1)}, u32[]{:S(2)}) copy-start(bf16[256,128]{1,0:T(8,128)(2,1)} %param.17) | copy-start | bytes 196612
  70.7 98.5 %copy-start.5 = (f32[1024]{0:T(1024)S(1)}, f32[1024]{0:T(1024)}, u32[]{:S(2)}) copy-start(f32[1024]{0:T(1024)} %param.23) | copy-start | bytes 12292
  121.6 49.7 %copy-start.7 = (u32[32]{0:T(128)S(1)}, u32[32]{0:T(128)}, u32[]{:S(2)}) copy-start(u32[32]{0:T(128)} %constant.56) | copy-start | bytes 388
  122.7 71.3 %reduce-scatter.16.cloned.1.call-start = ((), (), s32[]{:S(2)}) async-start(), calls=%async_computation.9 | async-start | bytes 163840 | tf_op jit(solution)/shard_map/reduce_scatter | solution.py:69
  171.3 49.4 %reduce-scatter.18.cloned.1.call-start = ((), (), s32[]{:S(2)}) async-start(), calls=%async_computation.10 | async-start | bytes 163840 | tf_op jit(solution)/shard_map/reduce_scatter | solution.py:72
  174.6 73.6 %reduce-scatter.20.cloned.1.call-start = ((), (), s32[]{:S(2)}) async-start(), calls=%async_computation.11 | async-start | bytes 327680 | tf_op jit(solution)/shard_map/reduce_scatter | solution.py:75
  177.1 98.2 %reduce-scatter.14.cloned.1.call-start = ((), (), s32[]{:S(2)}) async-start(), calls=%async_computation.8 | async-start | bytes 327680 | tf_op jit(solution)/shard_map/reduce_scatter | solution.py:78
  189.5 130.2 %reduce-scatter.24.cloned.1.call-start = ((), (), s32[]{:S(2)}) async-start(), calls=%async_computation.16 | async-start | bytes 589824
  254.5 7.4 %copy-start.1 = (f32[64,4,64,128]{3,2,1,0:T(8,128)}, f32[64,4,64,128]{3,2,1,0:T(8,128)S(1)}, u32[]{:S(2)}) copy-start(f32[64,4,64,128]{3,2,1,0:T(8,128)S(1)} %multiply_add_fusion) | copy-start | bytes 25165828
  254.5 20.8 %copy-start.3 = (f32[512]{0:T(512)S(1)}, f32[512]{0:T(512)}, u32[]{:S(2)}) copy-start(f32[512]{0:T(512)} %param.28) | copy-start | bytes 6148
  261.8 72.9 %copy-start.6 = (f32[1024]{0:T(1024)S(1)}, f32[1024]{0:T(1024)}, u32[]{:S(2)}) copy-start(f32[1024]{0:T(1024)} %param.30) | copy-start | bytes 12292
  288.3 90.4 %all-gather.7.cloned.1.call-start = ((), (), s32[]{:S(2)}) async-start(), calls=%async_computation.14 | async-start | bytes 3604480 | tf_op jit(solution)/shard_map/all_gather | solution.py:42
  338.4 90.9 %all-reduce.6.cloned.1.call-start = ((), (), s32[]{:S(2)}) async-start(), calls=%async_computation.12 | async-start | bytes 1441792 | tf_op jit(solution)/shard_map/psum | solution.py:41
  342.2 123.1 %reduce-scatter.26.cloned.1.call-start = ((), (), s32[]{:S(2)}) async-start(), calls=%async_computation.17 | async-start | bytes 589824
Sparse Core Ops, SparseCore 0:
  25.8 41.5 all-gather.4
  70.4 47.6 all-reduce.3
  122.8 31.3 reduce-scatter.21
  171.4 22.4 reduce-scatter.15
  196.5 24.1 reduce-scatter.17
  223.9 24.2 reduce-scatter.19
  250.9 24.3 reduce-scatter.13
  288.4 31.3 reduce-scatter.23
  338.6 40.0 all-gather.6
  381.6 47.6 all-reduce.5
  433.9 31.3 reduce-scatter.25
